TPU v7x, 512 devices: a whole 4x4x16 slice. The times are simulated.
512 devices in a mesh: rep: 2 (over z_hi), fs: 32 (over z_lo, y), tp: 8 (over x, core).
Axes of the slice: x: 4, y: 4, z: 16 (z_hi: 2, z_lo: 8; z = z_hi * 8 + z_lo), core: 2. Of those that a mesh axis runs over, the one named last changes fastest.
Arguments:
- tokens: bfloat16 [49152, 2048], P(('rep', 'fs', 'tp')), may hold values from -6 to 6
- norm_gain: float32 [2048], replicated, may hold values from 0.1 to 1.9
- gate_weight: float32 [2048, 5632], P('fs', 'tp'), may hold values from -0.125 to 0.125
- up_weight: float32 [2048, 5632], P('fs', 'tp'), may hold values from -0.125 to 0.125
- gate_scale: float32 [5632], P('tp'), may hold values from 0.3 to 3
- up_scale: float32 [5632], P('tp'), may hold values from 0.3 to 3
- down_weight: float32 [5632, 2048], P('tp', 'fs'), may hold values from -0.078125 to 0.078125
- down_scale: float32 [2048], replicated, may hold values from 0.3 to 3
Outputs:
- mixed: bfloat16 [49152, 2048], P(('rep', 'fs', 'tp'))
All inputs are finite; a program needn't handle non-finite values.
Results may differ from a plain program's by a relative error of at most 0.014.
Values may be sent and summed in bfloat16 or wider, within the bound.
A program may use at most 64 MiB of HBM per device.

v0:
```python
import jax
import jax.numpy as jnp
from jax import lax
from jax.sharding import PartitionSpec as P


def joined_along(blocks, dim):
    shape = list(blocks.shape[1:])
    shape[dim] *= blocks.shape[0]
    return jnp.moveaxis(blocks, 0, dim).reshape(shape)


def sent_to_all(shard, axis):
    size = lax.axis_size(axis)
    return lax.all_to_all(
        jnp.broadcast_to(shard[None], (size, *shard.shape)), axis, 0, 0, tiled=True
    )


def gather_directly(shard, axis, dim):
    return joined_along(sent_to_all(shard, axis), dim)


def in_one_piece(arrays, axis, dim, along):
    both = jnp.concatenate(arrays, axis=along)
    out, at, gathered = (lax.all_gather(both, axis, axis=dim, tiled=True), 0, [])
    for a in arrays:
        gathered.append(lax.slice_in_dim(out, at, at + a.shape[along], axis=along))
        at += a.shape[along]
    return tuple(gathered)


def cut_along(shard, dim, size):
    shape = shard.shape
    blocks = shard.reshape(*shape[:dim], size, shape[dim] // size, *shape[dim + 1 :])
    return jnp.moveaxis(blocks, dim, 0)


def sum_at_owner(shard, axis, dim):
    size = lax.axis_size(axis)
    blocks = lax.all_to_all(cut_along(shard, dim, size), axis, 0, 0, tiled=True)
    return jnp.sum(blocks.astype(jnp.float32), axis=0)


def on_device(
    tokens, norm_gain, gate_weight, up_weight, gate_scale, up_scale, down_weight, down_scale
):
    values = tokens.astype(jnp.float32)
    own_normed = (
        values * lax.rsqrt(jnp.mean(values * values, axis=-1, keepdims=True) + 1e-06) * norm_gain
    ).astype(jnp.bfloat16)
    normed = gather_directly(own_normed, "tp", 0)
    gate_local = gate_weight.astype(jnp.bfloat16)
    up_local = up_weight.astype(jnp.bfloat16)
    gate_whole, up_whole = in_one_piece((gate_local, up_local), "fs", 0, 1)
    gate_value = jnp.dot(normed, gate_whole, preferred_element_type=jnp.float32)
    up_value = jnp.dot(normed, up_whole, preferred_element_type=jnp.float32)
    hidden = (jax.nn.silu(gate_value * gate_scale) * (up_value * up_scale)).astype(jnp.bfloat16)
    partial_value = jnp.dot(
        hidden,
        lax.all_gather(down_weight.astype(jnp.bfloat16), "fs", axis=1, tiled=True),
        preferred_element_type=jnp.float32,
    )
    partial_value = partial_value.astype(jnp.bfloat16).astype(jnp.float32)
    summed = sum_at_owner(partial_value.astype(jnp.bfloat16), "tp", 0)
    return (summed * down_scale).astype(jnp.bfloat16)


def solution(mesh):
    placed = (
        P(("rep", "fs", "tp"), None),
        P(),
        P("fs", "tp"),
        P("fs", "tp"),
        P("tp"),
        P("tp"),
        P("tp", "fs"),
        P(),
    )
    return jax.shard_map(
        on_device,
        mesh=mesh,
        in_specs=placed,
        out_specs=P(("rep", "fs", "tp"), None),
        check_vma=False,
    )
```

profile of v0, /device:TPU:1, one launch (start us, length us, event | category | flops | bytes accessed | tf_op | source)
XLA Modules:
  0.0 533.2 jit_solution(5803203277212147337)
XLA Ops:
  6.5 0.0 all-gather.3.cloned.1.call-start
  6.5 0.9 convert_element_type.31
  7.5 0.9 convert_element_type.32
  8.4 0.8 pad_maximum_fusion
  9.2 0.0 all-gather.3.cloned.1.call-update
  9.2 0.0 all-gather.5.cloned.1.call-start
  9.3 1.6 convert_element_type.34
  10.8 0.0 all-gather.5.cloned.1.call-update
  10.9 1.2 fusion.11
  12.1 1.2 fusion.13
  13.2 0.4 broadcast_in_dim.2
  13.6 47.1 %all_to_all.10 = bf16[8,96,2048]{2,1,0:T(8,128)(2,1)S(1)} all-to-all(bf16[8,96,2048]{2,1,0:T(8,128)(2,1)S(1)} %broadcast_in_dim.2), channel_id=1, replica_groups=mesh['rep'=2,'fs'=32,'tp'=8] {'tp'}, dimensions={0} | all-to-all | bytes 6291456 | tf_op jit(solution)/shard_map/all_to_all | solution.py:15
  60.7 165.4 %all-gather.3.cloned.1.call-done = bf16[2048,1408]{1,0:T(8,128)(2,1)} async-done(((bf16[64,1408]{1,0:T(8,128)(2,1)}), bf16[2048,1408]{1,0:T(8,128)(2,1)}) %all-gather.3.cloned.1.call-update) | async-done | bytes 5767184 | tf_op jit(solution)/shard_map/all_gather | solution.py:26
  226.1 0.0 copy-start.1
  226.1 0.0 copy-start.2
  226.1 6.8 %fusion = f32[768,704]{0,1:T(8,128)} fusion(bf16[768,2048]{1,0:T(8,128)(2,1)S(1)} %bitcast.5, bf16[2048,1408]{1,0:T(8,128)(2,1)} %all-gather.3.cloned.1.call-done), kind=kOutput, calls=%fused_computation.2 | convolution fusion | flops 2214592512 | bytes 8454144 | tf_op jit(solution)/shard_map/dot_general | solution.py:57
  232.8 215.9 %all-gather.5.cloned.1.call-done = bf16[704,2048]{0,1:T(8,128)(2,1)} async-done(((bf16[704,64]{0,1:T(8,128)(2,1)}), bf16[704,2048]{0,1:T(8,128)(2,1)}) %all-gather.5.cloned.1.call-update) | async-done | bytes 2883600 | tf_op jit(solution)/shard_map/all_gather | solution.py:61
  448.7 0.0 copy-done.1
  448.7 0.0 copy-done.2
  448.7 11.7 %convolution_convert_fusion = bf16[768,2048]{1,0:T(8,128)(2,1)} fusion(bf16[704,2048]{0,1:T(8,128)(2,1)} %all-gather.5.cloned.1.call-done, f32[768,704]{0,1:T(8,128)} %fusion, bf16[768,2048]{1,0:T(8,128)(2,1)S(1)} %bitcast.6, bf16[2048,1408]{1,0:T(8,128)(2,1)} %all-gather.3.cloned.1.call-done, f32[704]{0:T(1024)S(1)} %copy-done.1, f32[704]{0:T(1024)S(1)} %copy-done.2), kind=kOutput, calls=%fused_computation.1 | convolution fusion | flops 4435083264 | bytes 14751232 | tf_op jit(solution)/shard_map/dot_general | solution.py:59
  460.4 64.4 %all_to_all.11 = bf16[8,96,2048]{2,1,0:T(8,128)(2,1)S(1)} all-to-all(bf16[8,96,2048]{2,1,0:T(8,128)(2,1)} %bitcast.7), channel_id=1, replica_groups=mesh['rep'=2,'fs'=32,'tp'=8] {'tp'}, dimensions={0} | all-to-all | bytes 6291456 | tf_op jit(solution)/shard_map/all_to_all | solution.py:41
  524.9 0.6 convert_reduce_fusion
  525.4 0.1 copy-done
  525.6 0.8 multiply_convert_fusion.1
  (2 shorter events, 0.0 us)
Async XLA Ops:
  6.5 219.5 %all-gather.3.cloned.1.call-start = ((), (), s32[]{:S(2)}) async-start(), calls=%async_computation.2 | async-start | bytes 5947392 | tf_op jit(solution)/shard_map/all_gather | solution.py:26
  9.2 439.5 %all-gather.5.cloned.1.call-start = ((), (), s32[]{:S(2)}) async-start(), calls=%async_computation.3 | async-start | bytes 3244032 | tf_op jit(solution)/shard_map/all_gather | solution.py:61
  226.1 222.6 %copy-start.1 = (f32[704]{0:T(1024)S(1)}, f32[704]{0:T(1024)}, u32[]{:S(2)}) copy-start(f32[704]{0:T(1024)} %param.13) | copy-start | bytes 8452
  226.1 222.6 %copy-start.2 = (f32[704]{0:T(1024)S(1)}, f32[704]{0:T(1024)}, u32[]{:S(2)}) copy-start(f32[704]{0:T(1024)} %param.12) | copy-start | bytes 8452
  524.9 0.7 copy-start
Sparse Core Ops, SparseCore 0:
  9.4 216.6 all-gather.2
  228.2 220.5 all-gather.4
where the time goes:
time: 534 us; the launch traced here: 533 us
  waiting for transfers between devices  381 us (71%)
  blocking collectives  112 us (21%)
  matrix products  18.5 us (3%)
  between operations  13.4 us (3%)
  other arithmetic  7.93 us (1%)
    all_gather x1, waiting for transfers between devices, on_device(): lax.all_gather(down_weight.astype(jnp.bfloat16), 'fs', axis=1, tiled=True)  216 us
    all_gather x1, waiting for transfers between devices, in_one_piece(): lax.all_gather(both, axis, axis=dim, tiled=True)  165 us
    all_to_all x1, blocking collectives, sum_at_owner(): blocks = lax.all_to_all(cut_along(shard, dim, size), axis, 0, 0, tiled=True)  64.4 us
    all_to_all x1, blocking collectives, sent_to_all(): lax.all_to_all(jnp.broadcast_to(shard[None], (size, *shard.shape)), axis,...  47.1 us
    dot_general x1, matrix products, on_device(): jnp.dot(hidden, lax.all_gather(down_weight.astype(jnp.bfloat16), 'fs', ax...  11.7 us
  transfers between devices with their start and end apart: 2, of which 2 were waited for; matrix products, arithmetic and copies ran while one was open for 2% of the time, Pallas kernels for 0%

commit v1 on v0

v1 whole, which is shorter than its diff:
```python
import jax
import jax.numpy as jnp
from jax import lax
from jax.experimental import pallas as pl
from jax.experimental.pallas import tpu as pltpu
from jax.sharding import PartitionSpec as P

BF16 = jnp.bfloat16
F32 = jnp.float32
D = 2048
ROWS = 96
ALL_ROWS = 768
NZ, NY, NX = 8, 4, 4
WA, WB = 640, 768
DA, DK = 256, 768

ICI = 45e3
SIB = 500e3
LAT = 2.0
LAT_SIB = 1.0
ISSUE = 0.06
BACKLOG = 3.0
T_MM_A, T_MM_B, T_SILU, T_DN = 0.6, 0.7, 2.5, 0.7
T_RED1, T_RED2, T_FIN = 0.3, 0.2, 0.2


class Send:
    def __init__(self, link, src, dst, nbytes, deps, prio, after=0.0):
        self.link, self.src, self.dst, self.nbytes = link, src, dst, nbytes
        self.deps, self.prio, self.after = deps, prio, after
        self.idx = None


class Task:
    def __init__(self, kind, unit, deps, gives, dur, prio):
        self.kind, self.unit, self.deps, self.gives = kind, unit, deps, gives
        self.dur, self.prio = dur, prio


def weight_sends(name, first, width, p1, p2, after):
    sends = []
    nb = 64 * width * 2
    whole, lo, hi = (0, 64), (0, 32), (32, 32)

    def add(link, dz, dy, part, ddz, ddy, deps, prio):
        sends.append(
            Send(
                link,
                (name, dz % 8, dy % 4, part),
                (name, (dz + ddz) % 8, (dy + ddy) % 4, part),
                nb * part[1] // 64,
                deps,
                prio,
                after,
            )
        )

    def key(dz, dy, part):
        return (name, dz % 8, dy % 4, part)

    def avail(dz, dy):
        if (dz, dy) == (0, 0):
            return [("own", name)]
        halves = (dy == 2) if first == "y" else (dz == 4)
        if halves and (dz == 0 if first == "y" else dy == 0):
            return [key(dz, dy, lo), key(dz, dy, hi)]
        return [key(dz, dy, whole)]

    if first == "y":
        own = avail(0, 0)
        add("y+", 0, 0, whole, 0, -1, own, p1)
        add("y-", 0, 0, whole, 0, 1, own, p1)
        add("y+", 0, 3, lo, 0, -1, [key(0, 3, whole)], p1)
        add("y-", 0, 1, hi, 0, 1, [key(0, 1, whole)], p1)
        for dy in range(4):
            for dz in (0, 7, 6, 5):
                if dz != 5 or dy in (0, 1):
                    add("z+", dz, dy, whole, -1, 0, avail(dz, dy), p2)
            for dz in (0, 1, 2, 3):
                if dz != 3 or dy in (2, 3):
                    add("z-", dz, dy, whole, 1, 0, avail(dz, dy), p2)
    else:
        for dz in (0, 7, 6):
            add("z+", dz, 0, whole, -1, 0, avail(dz, 0), p1)
        add("z+", 5, 0, lo, -1, 0, avail(5, 0), p1)
        for dz in (0, 1, 2):
            add("z-", dz, 0, whole, 1, 0, avail(dz, 0), p1)
        add("z-", 3, 0, hi, 1, 0, avail(3, 0), p1)
        for dz in range(8):
            add("y+", dz, 0, whole, 0, -1, avail(dz, 0), p2)
            add("y-", dz, 0, whole, 0, 1, avail(dz, 0), p2)
            if dz in (0, 6, 2, 4):
                add("y+", dz, 3, whole, 0, -1, avail(dz, 3), p2 - 0.1)
            else:
                add("y-", dz, 1, whole, 0, 1, avail(dz, 1), p2 - 0.1)
    return sends


def unit_keys(name, first, dz):
    whole, lo, hi = (0, 64), (0, 32), (32, 32)
    keys = []
    for dy in range(4):
        if (dz, dy) == (0, 0):
            keys.append(("own", name))
        elif first == "y" and dz == 0 and dy == 2 or first == "z" and dy == 0 and dz == 4:
            keys += [(name, dz, dy, lo), (name, dz, dy, hi)]
        else:
            keys.append((name, dz, dy, whole))
    return keys


def build():
    sends, tasks = [], []
    tasks.append(Task("prep", 0, [], [("own", n) for n in ("A", "B", "DA", "DB")], 1.0, -2))
    tasks.append(Task("norm", 0, [], [("own", "X")], 1.0, -1))
    sends += weight_sends("B", "z", WB, 0, 2, 0.0)
    sends += weight_sends("A", "y", WA, 0, 2, 0.0)
    sends += weight_sends("DB", "z", DK - DA, 1, 3, 8.0)
    sends += weight_sends("DA", "y", DA, 1, 3, 8.0)

    xb = 48 * D * 2
    ox = [("own", "X")]
    sends.append(Send("s", ("X", 0, 0, 2), ("X", 1, 0, 2), 2 * xb, ox, 0))
    for h in (0, 1):
        sends.append(Send("x+", ("X", 0, 0, h), ("X", 0, 3, h), xb, ox, h))
        sends.append(Send("x-", ("X", 0, 0, 1 - h), ("X", 0, 1, 1 - h), xb, ox, h))
    sends.append(Send("x+", ("X", 0, 3, 0), ("X", 0, 2, 0), xb, [("X", 0, 3, 0)], 0))
    sends.append(Send("x-", ("X", 0, 1, 1), ("X", 0, 2, 1), xb, [("X", 0, 1, 1)], 0))
    xkeys = [("own", "X"), ("X", 1, 0, 2)]
    for dx in (1, 2, 3):
        for h in (0, 1):
            sends.append(Send("s", ("X", 0, dx, h), ("X", 1, dx, h), xb, [("X", 0, dx, h)], 0))
            xkeys += [("X", 0, dx, h), ("X", 1, dx, h)]

    done = []
    for u in range(8):
        for n, first, dur in (("A", "y", T_MM_A), ("B", "z", T_MM_B)):
            tasks.append(
                Task("mm" + n, u, xkeys + unit_keys(n, first, u), [("mm", n, u)], dur, 5)
            )
            done.append(("mm", n, u))
    tasks.append(Task("silu", 0, done, [("H",)], T_SILU, 5))
    for u in range(8):
        dk = [("H",)] + unit_keys("DA", "y", u) + unit_keys("DB", "z", u)
        tasks.append(Task("dn", u, dk, [("P", u)], T_DN, 5))
        sends.append(Send("s", ("S", u), ("S", u), 4 * 96 * 256 * 2, [("P", u)], 0))
        tasks.append(Task("red1", u, [("P", u), ("S", u)], [("T", u)], T_RED1, 4))
        sends.append(Send("x-", ("T", u, 0), ("R", u, 0), 48 * 512, [("T", u)], 0))
        sends.append(Send("x+", ("T", u, 1), ("R", u, 1), 48 * 512, [("T", u)], 0))
        tasks.append(
            Task("red2", u, [("T", u), ("R", u, 0), ("R", u, 1)], [("N", u)], T_RED2, 3)
        )
        sends.append(Send("x-", ("N", u, 0), ("F", u, 0), 96 * 512, [("N", u)], 0))
        sends.append(Send("x+", ("N", u, 1), ("F", u, 1), 96 * 512, [("N", u)], 0))
        tasks.append(Task("fin", u, [("N", u), ("F", u, 0), ("F", u, 1)], [("O", u)], T_FIN, 2))
    return sends, tasks


def schedule():
    sends, tasks = build()
    for i, s in enumerate(sends):
        s.idx = i
    known, free, order = {}, {}, []
    t, left = 0.0, list(sends) + list(tasks)
    while left:
        best, soonest = None, None
        for o in left:
            if any(k not in known for k in o.deps):
                continue
            at = max([known[k] for k in o.deps], default=0.0)
            if isinstance(o, Send):
                at = max(at, o.after, free.get(o.link, 0.0) - BACKLOG)
                rank = (0, o.prio, at)
            else:
                rank = (1, o.prio, at)
            if at <= t + 1e-9:
                if best is None or rank < best[0]:
                    best = (rank, o)
            elif soonest is None or at < soonest:
                soonest = at
        if best is None:
            t = soonest
            continue
        o = best[1]
        left.remove(o)
        order.append((t, o))
        if isinstance(o, Send):
            t += ISSUE
            rate, lat = (SIB, LAT_SIB) if o.link == "s" else (ICI, LAT)
            free[o.link] = max(free.get(o.link, 0.0), t) + o.nbytes / rate
            known[o.dst] = free[o.link] + lat
        else:
            t += o.dur
            for k in o.gives:
                known[k] = t
    return sends, order, t


SENDS, ORDER, END = schedule()


def nt(a, b):
    return lax.dot_general(a, b, (((1,), (1,)), ((), ())), preferred_element_type=F32)


def kernel(
    tok, gain, gw, uw, gsc, usc, dw, dsc, out,
    xbuf, wa, wb, dbuf, acca, accb, hid, pown, ssend, srecv, tsend, rrecv, nsend, frecv,
    send_sems, recv_sems,
):
    rep, fs, tp = lax.axis_index("rep"), lax.axis_index("fs"), lax.axis_index("tp")
    zlo, y = fs // NY, fs % NY
    zg = rep * NZ + zlo
    x, c = tp // 2, tp % 2

    def zn(step):
        to = (zg + step + 16) % 16
        return (to // NZ, (to % NZ) * NY + y, tp)

    def yn(step):
        return (rep, zlo * NY + (y + step + NY) % NY, tp)

    def xn(step):
        return (rep, fs, ((x + step + NX) % NX) * 2 + c)

    peer = {
        "z+": zn(1), "z-": zn(-1), "y+": yn(1), "y-": yn(-1),
        "x+": xn(1), "x-": xn(-1), "s": (rep, fs, x * 2 + 1 - c),
    }
    barrier = pltpu.get_barrier_semaphore()
    for p in peer.values():
        pl.semaphore_signal(barrier, inc=1, device_id=p, device_id_type=pl.DeviceIdType.MESH)

    yrow = [pl.multiple_of(((y + dy) % NY) * 64, 64) for dy in range(NY)]

    def place(key):
        name = key[0]
        if name in ("A", "B", "DA", "DB"):
            _, dz, dy, (at, n) = key
            rows = pl.ds(yrow[dy] + at, n)
            if name == "A":
                return wa.at[dz, rows, :]
            if name == "B":
                return wb.at[dz, rows, :]
            if name == "DA":
                return dbuf.at[dz, rows, pl.ds(0, DA)]
            return dbuf.at[dz, rows, pl.ds(DA, DK - DA)]
        if name == "X":
            _, s, dx, h = key
            base = (s * 4 + dx) * ROWS
            return xbuf.at[:, pl.ds(base, ROWS) if h == 2 else pl.ds(base + h * 48, 48), :]
        if name == "T":
            return tsend.at[key[1], key[2]]
        if name == "R":
            return rrecv.at[key[1], key[2]]
        if name == "N":
            return nsend.at[key[1], key[2]]
        return frecv.at[key[1], key[2]]

    def outgoing(s):
        if s.src[0] == "S":
            src, dst = ssend.at[s.src[1]], srecv.at[s.src[1]]
        else:
            src, dst = place(s.src), None
            if s.dst[0] in ("A", "B", "DA", "DB"):
                name, dz, _, _ = s.dst
                _, _, dy, (at, n) = s.src
                rows = pl.ds(yrow[dy] + at, n)
                if name == "A":
                    dst = wa.at[dz, rows, :]
                elif name == "B":
                    dst = wb.at[dz, rows, :]
                elif name == "DA":
                    dst = dbuf.at[dz, rows, pl.ds(0, DA)]
                else:
                    dst = dbuf.at[dz, rows, pl.ds(DA, DK - DA)]
            else:
                dst = place(s.dst)
        return pltpu.make_async_remote_copy(
            src_ref=src, dst_ref=dst, send_sem=send_sems.at[s.idx], recv_sem=recv_sems.at[s.idx],
            device_id=peer[s.link], device_id_type=pl.DeviceIdType.MESH,
        )

    by_dst = {s.dst: s for s in SENDS}
    waited = set()

    def arrive(key):
        if key in waited or key not in by_dst:
            return
        waited.add(key)
        s = by_dst[key]
        ref = srecv.at[key[1]] if key[0] == "S" else place(key)
        pltpu.make_async_remote_copy(
            src_ref=ref, dst_ref=ref, send_sem=send_sems.at[s.idx], recv_sem=recv_sems.at[s.idx],
            device_id=peer[s.link], device_id_type=pl.DeviceIdType.MESH,
        ).wait_recv()

    first = {"A": True, "B": True}

    def run(o):
        u = o.unit
        if o.kind == "prep":
            mine = pl.ds(yrow[0], 64)
            g, v = gw[...], uw[...]
            wa[0, mine, :] = g[:, :WA].astype(BF16)
            wb[0, mine, pl.ds(0, WA)] = v[:, :WA].astype(BF16)
            mixed = jnp.concatenate([g[:, WA:], v[:, WA:]], axis=1)
            wb[0, mine, pl.ds(WA, 128)] = mixed.astype(BF16)
            dt = dw[...].T
            dbuf[0, mine, pl.ds(0, WA)] = dt[:, :WA].astype(BF16)
            tail = jnp.concatenate([dt[:, WA:], jnp.zeros((64, 64), F32)], axis=1)
            dbuf[0, mine, pl.ds(WA, 128)] = tail.astype(BF16)
            pl.semaphore_wait(barrier, 7)
        elif o.kind == "norm":
            v = tok[...].astype(F32)
            r = lax.rsqrt(jnp.mean(v * v, axis=-1, keepdims=True) + 1e-06)
            n = (v * r * gain[...]).astype(BF16)
            for k in range(NZ):
                xbuf[(k - zlo + NZ) % NZ, pl.ds(0, ROWS), :] = n[:, k * 256 : (k + 1) * 256]
        elif o.kind in ("mmA", "mmB"):
            n = o.kind[2]
            w, acc = (wa, acca) if n == "A" else (wb, accb)
            start, first[n] = first[n], False

            @pl.loop(0, 3)
            def _(i):
                rows = pl.ds(pl.multiple_of(i * 256, 256), 256)
                part = jnp.dot(xbuf[u, rows, :], w[u], preferred_element_type=F32)
                acc[rows, :] = part if start else acc[rows, :] + part
        elif o.kind == "silu":
            gs, us = gsc[...], usc[...]
            mixed_scale = jnp.concatenate([gs[:, WA:], us[:, WA:]], axis=1)
            low = lax.broadcasted_iota(jnp.int32, (32, 128), 1) < 64

            @pl.loop(0, ALL_ROWS // 32)
            def _(i):
                rows = pl.ds(pl.multiple_of(i * 32, 32), 32)
                g = acca[rows, :] * gs[:, :WA]
                v = accb[rows, pl.ds(0, WA)] * us[:, :WA]
                hid[rows, pl.ds(0, WA)] = (g / (1.0 + jnp.exp(-g)) * v).astype(BF16)
                m = accb[rows, pl.ds(WA, 128)] * mixed_scale
                h = m / (1.0 + jnp.exp(-m)) * pltpu.roll(m, 64, 1)
                hid[rows, pl.ds(WA, 128)] = jnp.where(low, h, 0.0).astype(BF16)
        elif o.kind == "dn":
            ssend[u] = nt(hid[pl.ds(384, 384), :], dbuf[u]).astype(BF16)
            pown[u] = nt(hid[pl.ds(0, 384), :], dbuf[u])
        elif o.kind == "red1":
            q = pown[u] + srecv[u].astype(F32)
            pown[u] = q
            tsend[u, 0] = q[192:240].astype(BF16)
            tsend[u, 1] = q[240:288].astype(BF16)
        elif o.kind == "red2":
            r0, r1 = rrecv[u, 0].astype(F32), rrecv[u, 1].astype(F32)
            nsend[u, 0, pl.ds(0, 48), :] = (pown[u, pl.ds(288, 48), :] + r0).astype(BF16)
            nsend[u, 0, pl.ds(48, 48), :] = pown[u, pl.ds(336, 48), :].astype(BF16)
            nsend[u, 1, pl.ds(0, 48), :] = pown[u, pl.ds(96, 48), :].astype(BF16)
            nsend[u, 1, pl.ds(48, 48), :] = (pown[u, pl.ds(144, 48), :] + r1).astype(BF16)
        elif o.kind == "fin":
            total = pown[u, pl.ds(0, 96), :] + frecv[u, 0].astype(F32) + frecv[u, 1].astype(F32)
            cols = pl.ds(pl.multiple_of(((zlo + u) % NZ) * 256, 256), 256)
            out[:, cols] = (total * dsc[:, cols]).astype(BF16)

    for _, o in ORDER:
        for k in o.deps:
            arrive(k)
        if isinstance(o, Send):
            outgoing(o).start()
        else:
            run(o)
    for s in SENDS:
        outgoing(s).wait_send()


def on_device(
    tokens, norm_gain, gate_weight, up_weight, gate_scale, up_scale, down_weight, down_scale
):
    n = len(SENDS)
    vm = pl.BlockSpec(memory_space=pltpu.VMEM)
    return pl.pallas_call(
        kernel,
        out_shape=jax.ShapeDtypeStruct((ROWS, D), BF16),
        in_specs=[vm] * 8,
        out_specs=vm,
        scratch_shapes=[
            pltpu.VMEM((8, ALL_ROWS, 256), BF16),
            pltpu.VMEM((8, 256, WA), BF16),
            pltpu.VMEM((8, 256, WB), BF16),
            pltpu.VMEM((8, 256, DK), BF16),
            pltpu.VMEM((ALL_ROWS, WA), F32),
            pltpu.VMEM((ALL_ROWS, WB), F32),
            pltpu.VMEM((ALL_ROWS, DK), BF16),
            pltpu.VMEM((8, 384, 256), F32),
            pltpu.VMEM((8, 384, 256), BF16),
            pltpu.VMEM((8, 384, 256), BF16),
            pltpu.VMEM((8, 2, 48, 256), BF16),
            pltpu.VMEM((8, 2, 48, 256), BF16),
            pltpu.VMEM((8, 2, 96, 256), BF16),
            pltpu.VMEM((8, 2, 96, 256), BF16),
            pltpu.SemaphoreType.DMA((n,)),
            pltpu.SemaphoreType.DMA((n,)),
        ],
        compiler_params=pltpu.CompilerParams(
            collective_id=0, has_side_effects=True, vmem_limit_bytes=60 * 1024 * 1024
        ),
    )(
        tokens, norm_gain[None], gate_weight, up_weight, gate_scale[None], up_scale[None],
        down_weight, down_scale[None],
    )


def solution(mesh):
    placed = (
        P(("rep", "fs", "tp"), None),
        P(),
        P("fs", "tp"),
        P("fs", "tp"),
        P("tp"),
        P("tp"),
        P("tp", "fs"),
        P(),
    )
    return jax.shard_map(
        on_device,
        mesh=mesh,
        in_specs=placed,
        out_specs=P(("rep", "fs", "tp"), None),
        check_vma=False,
    )
```

time: 534 us -> 92.7 us (0.17)
  waiting for transfers between devices: 381 us -> 0 us
  blocking collectives: 112 us -> 0 us
  Pallas kernels: 0 us -> 86.9 us
  matrix products: 18.5 us -> 0 us
  between operations: 13.4 us -> 0.01 us
  other arithmetic: 7.93 us -> 0 us
    all_gather x2 -> x0, waiting for transfers between devices: 381 us -> none  [the longest x1 216 us: on_device(): lax.all_gather(down_weight.astype(jnp.bfloat16), 'fs', axis=1, tiled=True)]
    all_to_all x2 -> x0, blocking collectives: 112 us -> none  [the longest x1 64.4 us: sum_at_owner(): blocks = lax.all_to_all(cut_along(shard, dim, size), axis, 0, 0, tiled=True)]
    pallas_call x0 -> x1, Pallas kernels: none -> 86.9 us  [on_device(): pl.pallas_call(kernel, out_shape=jax.ShapeDtypeStruct((ROWS, D), BF16), i...]
    dot_general x2 -> x0, matrix products: 18.5 us -> none  [the longest x1 11.7 us: on_device(): jnp.dot(hidden, lax.all_gather(down_weight.astype(jnp.bfloat16), 'fs', ax...]
    convert_element_type x5 -> x0, other arithmetic: 5.42 us -> none  [the longest x1 1.57 us: on_device(): down_weight.astype(jnp.bfloat16)]
  transfers between devices with their start and end apart: 2 -> 0, of which waited for: 2 -> 0; matrix products, arithmetic and copies ran while one was open for 2% -> 0% of each run, Pallas kernels for 0% -> 0%
where the time goes in v1:
time: 92.7 us; the launch traced here: 92.4 us
  Pallas kernels  86.9 us (94%)
  local copies, waits for them, and re-layouts  5.49 us (6%)
    pallas_call x1, Pallas kernels, on_device(): pl.pallas_call(kernel, out_shape=jax.ShapeDtypeStruct((ROWS, D), BF16), i...  86.9 us
    unnamed x4, local copies, waits for them, and re-layouts  3.6 us

profile of v1, /device:TPU:1, one launch (start us, length us, event | category | flops | bytes accessed | tf_op | source)
XLA Modules:
  0.0 92.4 jit_solution(187162435015526409)
XLA Ops:
  0.0 0.0 copy-start
  0.0 1.3 %broadcast_in_dim.13.gsc = f32[1,704]{1,0:T(1,128)} reshape(f32[704]{0:T(1024)} %param.12) | data formatting | bytes 5632 | tf_op jit(solution)/shard_map/broadcast_in_dim | solution.py:406
  1.3 0.0 copy-done
  1.3 0.6 broadcast_in_dim.14.usc
  1.9 1.8 %copy.9.dw = f32[704,64]{1,0:T(8,128)} copy(f32[704,64]{0,1:T(8,128)} %param.14) | data formatting | bytes 360448 | tf_op args[6]
  3.7 86.9 %shard_map.82 = bf16[96,2048]{1,0:T(8,128)(2,1)} custom-call(bf16[96,2048]{1,0:T(8,128)(2,1)} %tok.1, f32[1,2048]{1,0:T(1,128)} %bitcast.2, f32[64,704]{1,0:T(8,128)} %gw.1, f32[64,704]{1,0:T(8,128)} %uw.1, f32[1,704]{1,0:T(1,128)} %broadcast_in_dim.13.gsc, f32[1,704]{1,0:T(1,128)} %broadcast_in_dim.14.usc, f32[704,64]{1,0:T(8,128)} %copy.9.dw, ...), custom_call_target="tpu_custom_call" | custom-call | tf_op jit(solution)/shard_map/pallas_call | solution.py:379
  90.6 1.8 %copy.11 = bf16[96,2048]{1,0:T(8,128)(2,1)} copy(bf16[96,2048]{1,0:T(8,128)(2,1)} %shard_map.82) | data formatting | bytes 786432
Async XLA Ops:
  0.0 1.3 %copy-start = (f32[704]{0:T(1024)S(1)}, f32[704]{0:T(1024)}, u32[]{:S(2)}) copy-start(f32[704]{0:T(1024)} %param.13) | copy-start | bytes 8452

commit v2 on v1

v2 whole, which is shorter than its diff:
```python
import jax
import jax.numpy as jnp
from jax import lax
from jax.experimental import pallas as pl
from jax.experimental.pallas import tpu as pltpu
from jax.sharding import PartitionSpec as P

BF16 = jnp.bfloat16
F32 = jnp.float32
D = 2048
ROWS = 96
ALL_ROWS = 768
NZ, NY, NX = 8, 4, 4
WA, WB = 640, 768
DK = 768
SLOTS = 6

ICI, SIB = 45e3, 500e3
LAT, LAT_SIB = 2.3, 1.0
ISSUE, BACKLOG = 0.06, 1.5
COST = {
    "prep": 0.4, "norm": 0.5, "mmA": 0.35, "mmB": 0.4, "silu": 1.7, "dn": 0.4,
    "red1": 0.15, "red2": 0.12, "fin": 0.12,
}


class Send:
    def __init__(self, link, src, dst, nbytes, deps, prio):
        self.link, self.src, self.dst, self.nbytes = link, src, dst, nbytes
        self.deps, self.prio = deps, prio
        self.slot = self.sem = None


class Task:
    def __init__(self, kind, unit, deps, gives, prio):
        self.kind, self.unit, self.deps, self.gives = kind, unit, deps, gives
        self.dur, self.prio = COST[kind], prio


def unit_keys(name, first, dz, dys=(0, 1, 2, 3)):
    keys = []
    for dy in dys:
        if (dz, dy) == (0, 0):
            keys.append(("own", name))
        elif (first == "y" and dz == 0 and dy == 2) or (first == "z" and dy == 0 and dz == 4):
            keys += [(name, dz, dy, "l"), (name, dz, dy, "h")]
        else:
            keys.append((name, dz, dy, "w"))
    return keys


def weight_sends(name, first, nbytes, p1, p2):
    sends = []

    def add(link, dz, dy, part, ddz, ddy, prio):
        deps = unit_keys(name, first, dz, (dy,))
        size = nbytes if part == "w" else nbytes // 2
        dst = (name, (dz + ddz) % NZ, (dy + ddy) % NY, part)
        sends.append(Send(link, (name, dz, dy, part), dst, size, deps, prio))

    if first == "y":
        add("y+", 0, 0, "w", 0, -1, p1)
        add("y-", 0, 0, "w", 0, 1, p1)
        add("y+", 0, 3, "l", 0, -1, p1)
        add("y-", 0, 1, "h", 0, 1, p1)
        for dy in range(4):
            for dz in (0, 7, 6, 5):
                if dz != 5 or dy in (0, 1):
                    add("z+", dz, dy, "w", -1, 0, p2)
            for dz in (0, 1, 2, 3):
                if dz != 3 or dy in (2, 3):
                    add("z-", dz, dy, "w", 1, 0, p2)
    else:
        for dz in (0, 7, 6, 5):
            add("z+", dz, 0, "l" if dz == 5 else "w", -1, 0, p1)
        for dz in (0, 1, 2, 3):
            add("z-", dz, 0, "h" if dz == 3 else "w", 1, 0, p1)
        for dz in range(NZ):
            add("y+", dz, 0, "w", 0, -1, p2)
            add("y-", dz, 0, "w", 0, 1, p2)
            if dz in (0, 6, 2, 4):
                add("y+", dz, 3, "w", 0, -1, p2 - 0.1)
            else:
                add("y-", dz, 1, "w", 0, 1, p2 - 0.1)
    return sends


def build():
    sends, tasks = [], []
    tasks.append(Task("prep", 0, [], [("own", n) for n in ("A", "B", "DA", "DB")], -2))
    tasks.append(Task("norm", 0, [], [("own", "X")], -1))
    sends += weight_sends("B", "z", 64 * WB * 2, 0, 2)
    sends += weight_sends("A", "y", 64 * WA * 2, 0, 2)
    sends += weight_sends("DB", "z", 224 * 256, 2.5, 3)
    sends += weight_sends("DA", "y", 128 * 256, 2.5, 3)

    xb = 48 * D * 2
    ox = [("own", "X")]
    sends.append(Send("s", ("X", 0, 0, 2), ("X", 1, 0, 2), 2 * xb, ox, 0))
    for h in (0, 1):
        sends.append(Send("x+", ("X", 0, 0, h), ("X", 0, 3, h), xb, ox, h))
        sends.append(Send("x-", ("X", 0, 0, 1 - h), ("X", 0, 1, 1 - h), xb, ox, h))
    sends.append(Send("x+", ("X", 0, 3, 0), ("X", 0, 2, 0), xb, [("X", 0, 3, 0)], 0))
    sends.append(Send("x-", ("X", 0, 1, 1), ("X", 0, 2, 1), xb, [("X", 0, 1, 1)], 0))
    xkeys = [("own", "X"), ("X", 1, 0, 2)]
    for dx in (1, 3, 2):
        got = [("X", 0, dx, 0), ("X", 0, dx, 1)]
        sends.append(Send("s", ("X", 0, dx, 2), ("X", 1, dx, 2), 2 * xb, got, 0))
        xkeys += got + [("X", 1, dx, 2)]

    done = []
    for u in range(NZ):
        for n, first in (("A", "y"), ("B", "z")):
            tasks.append(Task("mm" + n, u, xkeys + unit_keys(n, first, u), [("mm", n, u)], 5))
            done.append(("mm", n, u))
    tasks.append(Task("silu", 0, done, [("H",)], 5))
    for u in range(NZ):
        dk = [("H",)] + unit_keys("DA", "y", u) + unit_keys("DB", "z", u)
        tasks.append(Task("dn", u, dk, [("P", u)], 5))
        sends.append(Send("s", ("S", u), ("S", u), 4 * 96 * 256 * 2, [("P", u)], 0))
        tasks.append(Task("red1", u, [("P", u), ("S", u)], [("T", u)], 4))
        sends.append(Send("x-", ("T", u, 0), ("R", u, 0), 48 * 512, [("T", u)], 0))
        sends.append(Send("x+", ("T", u, 1), ("R", u, 1), 48 * 512, [("T", u)], 0))
        tasks.append(Task("red2", u, [("T", u), ("R", u, 0), ("R", u, 1)], [("N", u)], 3))
        sends.append(Send("x-", ("N", u, 0), ("F", u, 0), 96 * 512, [("N", u)], 0))
        sends.append(Send("x+", ("N", u, 1), ("F", u, 1), 96 * 512, [("N", u)], 0))
        tasks.append(Task("fin", u, [("N", u), ("F", u, 0), ("F", u, 1)], [("O", u)], 2))
    return sends, tasks


def greedy(ops):
    known, free, order, t, left = {}, {}, [], 0.0, list(range(len(ops)))
    while left:
        best, soonest = None, None
        for i in left:
            o = ops[i]
            if any(k not in known for k in o.deps):
                continue
            at = max([known[k] for k in o.deps], default=0.0)
            if isinstance(o, Send):
                at = max(at, free.get(o.link, 0.0) - BACKLOG)
                rank = (0, o.prio, at)
            else:
                rank = (1, o.prio, at)
            if at <= t + 1e-9:
                if best is None or rank < best[0]:
                    best = (rank, i)
            elif soonest is None or at < soonest:
                soonest = at
        if best is None:
            t = soonest
            continue
        o = ops[best[1]]
        left.remove(best[1])
        order.append(best[1])
        if isinstance(o, Send):
            t += ISSUE
            rate, lat = (SIB, LAT_SIB) if o.link == "s" else (ICI, LAT)
            free[o.link] = max(free.get(o.link, 0.0), t) + o.nbytes / rate
            known[o.dst] = free[o.link] + lat
        else:
            t += o.dur
            for k in o.gives:
                known[k] = t
    return order


PLAN = (
    178, 0, 68, 97, 64, 32, 33, 96, 179, 129, 8, 4, 36, 9, 72, 128, 132, 40, 130, 73,
    100, 69, 1, 35, 99, 98, 34, 65, 5, 94, 131, 11, 93, 60, 12, 57, 41, 2, 53, 50,
    30, 10, 107, 27, 37, 90, 14, 135, 47, 134, 6, 75, 124, 133, 66, 78, 76, 43, 26, 24,
    61, 54, 79, 3, 13, 136, 58, 29, 51, 25, 92, 7, 31, 117, 48, 70, 137, 42, 62, 88,
    28, 183, 180, 23, 194, 38, 44, 18, 55, 95, 195, 59, 111, 20, 15, 52, 182, 16, 45, 63,
    19, 22, 21, 17, 39, 49, 114, 184, 81, 192, 185, 56, 104, 74, 71, 87, 125, 46, 112, 118,
    121, 181, 89, 67, 77, 193, 190, 80, 101, 186, 91, 191, 82, 189, 108, 115, 187, 188, 122, 105,
    196, 201, 143, 109, 84, 197, 138, 126, 225, 173, 119, 102, 221, 202, 144, 145, 123, 168, 205, 198,
    140, 148, 139, 113, 106, 83, 116, 226, 174, 110, 175, 85, 222, 169, 170, 206, 149, 150, 120, 127,
    86, 103, 203, 146, 147, 199, 141, 142, 217, 163, 227, 176, 177, 223, 209, 153, 218, 165, 164, 172,
    213, 158, 171, 207, 204, 210, 155, 200, 154, 214, 160, 152, 159, 151, 219, 166, 228, 167, 211, 224,
    157, 156, 215, 161, 162, 208, 220, 212, 216,
)
SENDS, TASKS = build()
OPS = SENDS + TASKS
ORDER = [OPS[i] for i in (PLAN or greedy(OPS))]


def number():
    links = ("y+", "y-", "z+", "z-", "x+", "x-", "s")
    count, sems = {}, {}
    for o in ORDER:
        if isinstance(o, Send):
            n = count.get(o.link, 0)
            count[o.link] = n + 1
            o.slot = links.index(o.link) * SLOTS + n % SLOTS
            group = o.dst[:2] if o.dst[0] in ("R", "F") else o.dst
            o.sem = sems.setdefault(group, len(sems))
    return len(links) * SLOTS, len(sems)


N_SEND, N_RECV = number()


def nt(a, b):
    return lax.dot_general(a, b, (((1,), (1,)), ((), ())), preferred_element_type=F32)


def kernel(
    tok_in, gain_in, gw_in, uw_in, gsc_in, usc_in, dw_in, dsc_in, out,
    tok, gain, gw, uw, gsc, usc, dw, dsc,
    xbuf, wa, wb, dbuf, acca, accb, hid, pown, ssend, srecv, tsend, rrecv, nsend, frecv,
    send_sems, recv_sems, in_sems,
):
    rep, fs, tp = lax.axis_index("rep"), lax.axis_index("fs"), lax.axis_index("tp")
    zlo, y = fs // NY, fs % NY
    zg = rep * NZ + zlo
    x, c = tp // 2, tp % 2

    def zn(step):
        to = (zg + step + 16) % 16
        return (to // NZ, (to % NZ) * NY + y, tp)

    def yn(step):
        return (rep, zlo * NY + (y + step + NY) % NY, tp)

    def xn(step):
        return (rep, fs, ((x + step + NX) % NX) * 2 + c)

    peer = {
        "z+": zn(1), "z-": zn(-1), "y+": yn(1), "y-": yn(-1),
        "x+": xn(1), "x-": xn(-1), "s": (rep, fs, x * 2 + 1 - c),
    }
    barrier = pltpu.get_barrier_semaphore()
    for p in peer.values():
        pl.semaphore_signal(barrier, inc=1, device_id=p, device_id_type=pl.DeviceIdType.MESH)

    loads = [
        pltpu.make_async_copy(a, b, in_sems.at[i])
        for i, (a, b) in enumerate(
            (
                (gw_in, gw), (uw_in, uw), (dw_in, dw), (tok_in, tok), (gain_in, gain),
                (gsc_in, gsc), (usc_in, usc), (dsc_in, dsc),
            )
        )
    ]
    for load in loads:
        load.start()

    yabs = [(y + dy) % NY for dy in range(NY)]
    parts = {
        "A": {"w": (0, 64), "l": (0, 32), "h": (32, 32)},
        "DA": {"w": (0, 128), "l": (0, 64), "h": (64, 64)},
        "DB": {"w": (128, 224), "l": (128, 112), "h": (240, 112)},
    }
    parts["B"] = parts["A"]

    def weight(name, dz, dy, part):
        at, n = parts[name][part]
        if name in ("A", "B"):
            rows = pl.ds(pl.multiple_of(yabs[dy] * 64 + at, 32), n)
            return (wa if name == "A" else wb).at[dz, rows, :]
        return dbuf.at[dz, yabs[dy], pl.ds(at, n), :]

    def place(key):
        name = key[0]
        if name in parts:
            return weight(*key)
        if name == "X":
            _, s, dx, h = key
            base = (s * 4 + dx) * ROWS
            return xbuf.at[:, pl.ds(base, ROWS) if h == 2 else pl.ds(base + h * 48, 48), :]
        if name == "T":
            return tsend.at[key[1], key[2]]
        if name == "R":
            return rrecv.at[key[1], key[2]]
        if name == "N":
            return nsend.at[key[1], key[2]]
        return frecv.at[key[1], key[2]]

    def copy(s, src, dst):
        return pltpu.make_async_remote_copy(
            src_ref=src, dst_ref=dst, send_sem=send_sems.at[s.slot], recv_sem=recv_sems.at[s.sem],
            device_id=peer[s.link], device_id_type=pl.DeviceIdType.MESH,
        )

    def outgoing(s):
        if s.src[0] == "S":
            return copy(s, ssend.at[s.src[1]], srecv.at[s.src[1]])
        if s.dst[0] in parts:
            name, dz, _, part = s.dst
            return copy(s, place(s.src), weight(name, dz, s.src[2], part))
        return copy(s, place(s.src), place(s.dst))

    by_dst = {s.dst: s for s in SENDS}
    waited = set()

    def arrive(key):
        if key not in by_dst:
            return
        s = by_dst[key]
        if s.sem in waited:
            return
        waited.add(s.sem)
        if key[0] == "S":
            ref = srecv.at[key[1]]
        elif key[0] in ("R", "F"):
            ref = (rrecv if key[0] == "R" else frecv).at[key[1]]
        else:
            ref = place(key)
        copy(s, ref, ref).wait_recv()

    first = {"A": True, "B": True}

    def run(o):
        u = o.unit
        if o.kind == "prep":
            for load in loads[:3]:
                load.wait()
            mine = pl.ds(pl.multiple_of(y * 64, 64), 64)
            g, v, dt = gw[...], uw[...], dw[...]
            wa[0, mine, :] = g[:, :WA].astype(BF16)
            wb[0, mine, pl.ds(0, WA)] = v[:, :WA].astype(BF16)
            mixed = jnp.concatenate([g[:, WA:], v[:, WA:]], axis=1)
            wb[0, mine, pl.ds(WA, 128)] = mixed.astype(BF16)
            for i in range(5):
                dbuf[0, y, pl.ds(i * 64, 64), :] = dt[:, i * 128 : (i + 1) * 128].astype(BF16)
            last = jnp.concatenate([dt[:32, WA:], dt[32:, WA:]], axis=1)
            dbuf[0, y, pl.ds(320, 32), :] = last.astype(BF16)
            pl.semaphore_wait(barrier, 7)
        elif o.kind == "norm":
            for load in loads[3:5]:
                load.wait()
            v = tok[...].astype(F32)
            r = lax.rsqrt(jnp.mean(v * v, axis=-1, keepdims=True) + 1e-06)
            n = (v * r * gain[...]).astype(BF16)
            for k in range(NZ):
                xbuf[(k - zlo + NZ) % NZ, pl.ds(0, ROWS), :] = n[:, k * 256 : (k + 1) * 256]
        elif o.kind in ("mmA", "mmB"):
            n = o.kind[2]
            w, acc = (wa, acca) if n == "A" else (wb, accb)
            start, first[n] = first[n], False

            part = jnp.dot(xbuf[u], w[u], preferred_element_type=F32)
            acc[...] = part if start else acc[...] + part
        elif o.kind == "silu":
            for load in loads[5:]:
                load.wait()
            gs, us = gsc[...].reshape(1, 704), usc[...].reshape(1, 704)
            mixed_scale = jnp.concatenate([gs[:, WA:], us[:, WA:]], axis=1)
            low = lax.broadcasted_iota(jnp.int32, (32, 128), 1) < 64

            @pl.loop(0, ALL_ROWS // 32)
            def _(i):
                rows = pl.ds(pl.multiple_of(i * 32, 32), 32)
                g = acca[rows, :] * gs[:, :WA]
                v = accb[rows, pl.ds(0, WA)] * us[:, :WA]
                hid[rows, pl.ds(0, WA)] = (g / (1.0 + jnp.exp(-g)) * v).astype(BF16)
                m = accb[rows, pl.ds(WA, 128)] * mixed_scale
                h = m / (1.0 + jnp.exp(-m)) * pltpu.roll(m, 64, 1)
                hid[rows, pl.ds(WA, 128)] = jnp.where(low, h, 0.0).astype(BF16)
        elif o.kind == "dn":
            tiles = [dbuf[u, :, pl.ds(i * 64, 64), :].reshape(256, 128) for i in range(5)]
            left = dbuf[u, :, pl.ds(320, 32), :]
            right = pltpu.roll(left.astype(F32).reshape(128, 128), 64, 1).astype(BF16)
            tiles.append(jnp.concatenate([left, right.reshape(4, 32, 128)], axis=1).reshape(256, 128))
            w = jnp.concatenate(tiles, axis=1)
            ssend[u] = nt(hid[pl.ds(384, 384), :], w).astype(BF16)
            pown[u] = nt(hid[pl.ds(0, 384), :], w)
        elif o.kind == "red1":
            q = pown[u] + srecv[u].astype(F32)
            pown[u] = q
            tsend[u, 0] = q[192:240].astype(BF16)
            tsend[u, 1] = q[240:288].astype(BF16)
        elif o.kind == "red2":
            r0, r1 = rrecv[u, 0].astype(F32), rrecv[u, 1].astype(F32)
            nsend[u, 0, pl.ds(0, 48), :] = (pown[u, pl.ds(288, 48), :] + r0).astype(BF16)
            nsend[u, 0, pl.ds(48, 48), :] = pown[u, pl.ds(336, 48), :].astype(BF16)
            nsend[u, 1, pl.ds(0, 48), :] = pown[u, pl.ds(96, 48), :].astype(BF16)
            nsend[u, 1, pl.ds(48, 48), :] = (pown[u, pl.ds(144, 48), :] + r1).astype(BF16)
        elif o.kind == "fin":
            total = pown[u, pl.ds(0, 96), :] + frecv[u, 0].astype(F32) + frecv[u, 1].astype(F32)
            cols = pl.ds(pl.multiple_of(((zlo + u) % NZ) * 256, 256), 256)
            out[:, cols] = (total * dsc[:, cols]).astype(BF16)

    sent = {}
    for o in ORDER:
        for key in o.deps:
            arrive(key)
        if isinstance(o, Send):
            if o.slot in sent:
                sent[o.slot].wait_send()
            sent[o.slot] = outgoing(o)
            sent[o.slot].start()
        else:
            run(o)
    for c_out in sent.values():
        c_out.wait_send()


def on_device(
    tokens, norm_gain, gate_weight, up_weight, gate_scale, up_scale, down_weight, down_scale
):
    hbm = pl.BlockSpec(memory_space=pl.ANY)
    vm = pl.BlockSpec(memory_space=pltpu.VMEM)
    return pl.pallas_call(
        kernel,
        out_shape=pltpu.VMEM((ROWS, D), BF16),
        in_specs=[hbm] * 8,
        out_specs=vm,
        scratch_shapes=[
            pltpu.VMEM((ROWS, D), BF16),
            pltpu.VMEM((1, D), F32),
            pltpu.VMEM((64, 704), F32),
            pltpu.VMEM((64, 704), F32),
            pltpu.VMEM((704,), F32),
            pltpu.VMEM((704,), F32),
            pltpu.VMEM((64, 704), F32),
            pltpu.VMEM((1, D), F32),
            pltpu.VMEM((8, ALL_ROWS, 256), BF16),
            pltpu.VMEM((8, 256, WA), BF16),
            pltpu.VMEM((8, 256, WB), BF16),
            pltpu.VMEM((8, 4, 352, 128), BF16),
            pltpu.VMEM((ALL_ROWS, WA), F32),
            pltpu.VMEM((ALL_ROWS, WB), F32),
            pltpu.VMEM((ALL_ROWS, DK), BF16),
            pltpu.VMEM((8, 384, 256), F32),
            pltpu.VMEM((8, 384, 256), BF16),
            pltpu.VMEM((8, 384, 256), BF16),
            pltpu.VMEM((8, 2, 48, 256), BF16),
            pltpu.VMEM((8, 2, 48, 256), BF16),
            pltpu.VMEM((8, 2, 96, 256), BF16),
            pltpu.VMEM((8, 2, 96, 256), BF16),
            pltpu.SemaphoreType.DMA((N_SEND,)),
            pltpu.SemaphoreType.DMA((N_RECV,)),
            pltpu.SemaphoreType.DMA((8,)),
        ],
        compiler_params=pltpu.CompilerParams(
            collective_id=0, has_side_effects=True, vmem_limit_bytes=60 * 1024 * 1024
        ),
    )(
        tokens, norm_gain[None], gate_weight, up_weight, gate_scale, up_scale,
        down_weight.T, down_scale[None],
    )


def solution(mesh):
    placed = (
        P(("rep", "fs", "tp"), None),
        P(),
        P("fs", "tp"),
        P("fs", "tp"),
        P("tp"),
        P("tp"),
        P("tp", "fs"),
        P(),
    )
    return jax.shard_map(
        on_device,
        mesh=mesh,
        in_specs=placed,
        out_specs=P(("rep", "fs", "tp"), None),
        check_vma=False,
    )
```

time: 92.7 us -> 77.6 us (0.84)
  Pallas kernels: 86.9 us -> 76.7 us
  local copies, waits for them, and re-layouts: 5.49 us -> 0.75 us
    pallas_call x1, Pallas kernels: 86.9 us -> 76.7 us  [on_device(): pl.pallas_call(kernel, out_shape=pltpu.VMEM((ROWS, D), BF16), in_specs=[h...]
    unnamed x4 -> x1, local copies, waits for them, and re-layouts: 3.6 us -> 0.75 us
    broadcast_in_dim x2 -> x0, local copies, waits for them, and re-layouts: 1.88 us -> none  [the longest x1 1.29 us: on_device(): gate_scale[None]]
where the time goes in v2:
time: 77.6 us; the launch traced here: 77.4 us
  Pallas kernels  76.7 us (99%)
    pallas_call x1, Pallas kernels, on_device(): pl.pallas_call(kernel, out_shape=pltpu.VMEM((ROWS, D), BF16), in_specs=[h...  76.7 us

profile of v2, /device:TPU:1, one launch (start us, length us, event | category | flops | bytes accessed | tf_op | source)
XLA Modules:
  0.0 77.4 jit_solution(7184589965446187648)
XLA Ops:
  0.0 76.7 %shard_map.82 = bf16[96,2048]{1,0:T(8,128)(2,1)S(1)} custom-call(bf16[96,2048]{1,0:T(8,128)(2,1)} %tok_in.1, f32[1,2048]{1,0:T(1,128)} %bitcast.4, f32[64,704]{1,0:T(8,128)} %gw_in.1, f32[64,704]{1,0:T(8,128)} %uw_in.1, f32[704]{0:T(1024)} %gsc_in.1, f32[704]{0:T(1024)} %usc_in.1, f32[64,704]{1,0:T(8,128)} %bitcast.3, f32[1,2048]{1,0:T(1,128)} %bitcast.5), custom_call_target="tpu_custom_call" | custom-call | tf_op jit(solution)/shard_map/pallas_call | solution.py:404
  76.7 0.7 copy.10

commit v3 on v2

--- a/solution.py
+++ b/solution.py
@@ -13,21 +13,34 @@
 NZ, NY, NX = 8, 4, 4
 WA, WB = 640, 768
 DK = 768
-SLOTS = 6
+LINKS = ("y+", "y-", "z+", "z-", "x+", "x-", "s")
+SLOT_COUNT = {l: 5 for l in LINKS}
 
 ICI, SIB = 45e3, 500e3
 LAT, LAT_SIB = 2.3, 1.0
 ISSUE, BACKLOG = 0.06, 1.5
 COST = {
-    "prep": 0.4, "norm": 0.5, "mmA": 0.35, "mmB": 0.4, "silu": 1.7, "dn": 0.4,
+    "prep": 0.4, "norm": 0.5, "mmA": 0.35, "mmB": 0.4, "silu": 0.6, "dns": 0.22, "dno": 0.22,
     "red1": 0.15, "red2": 0.12, "fin": 0.12,
 }
 
 
+TURN = {("A", 0): 3, ("A", 1): 0, ("B", 0): 4, ("DA", 0): 3, ("DA", 1): 4, ("DB", 0): 2}
+
+
+def ahead(name, dy):
+    return tuple(range(1, TURN[name, dy] + 1))
+
+
+def behind(name, dy):
+    n = TURN[name, dy]
+    return tuple(range(n - 1, 15)) if n else None
+
+
 class Send:
-    def __init__(self, link, src, dst, nbytes, deps, prio):
+    def __init__(self, link, src, dst, nbytes, deps, prio, only=None):
         self.link, self.src, self.dst, self.nbytes = link, src, dst, nbytes
-        self.deps, self.prio = deps, prio
+        self.deps, self.prio, self.only = deps, prio, only
         self.slot = self.sem = None
 
 
@@ -52,11 +65,11 @@
 def weight_sends(name, first, nbytes, p1, p2):
     sends = []
 
-    def add(link, dz, dy, part, ddz, ddy, prio):
+    def add(link, dz, dy, part, ddz, ddy, prio, only=None):
         deps = unit_keys(name, first, dz, (dy,))
         size = nbytes if part == "w" else nbytes // 2
         dst = (name, (dz + ddz) % NZ, (dy + ddy) % NY, part)
-        sends.append(Send(link, (name, dz, dy, part), dst, size, deps, prio))
+        sends.append(Send(link, (name, dz, dy, part), dst, size, deps, prio, only))
 
     if first == "y":
         add("y+", 0, 0, "w", 0, -1, p1)
@@ -66,15 +79,19 @@
         for dy in range(4):
             for dz in (0, 7, 6, 5):
                 if dz != 5 or dy in (0, 1):
-                    add("z+", dz, dy, "w", -1, 0, p2)
+                    add("z+", dz, dy, "w", -1, 0, p2, behind(name, dy) if dz == 5 else None)
             for dz in (0, 1, 2, 3):
                 if dz != 3 or dy in (2, 3):
                     add("z-", dz, dy, "w", 1, 0, p2)
+                else:
+                    add("z-", dz, dy, "w", 1, 0, p2, ahead(name, dy))
     else:
         for dz in (0, 7, 6, 5):
-            add("z+", dz, 0, "l" if dz == 5 else "w", -1, 0, p1)
+            only = behind(name, 0) if dz == 5 else None
+            add("z+", dz, 0, "l" if dz == 5 else "w", -1, 0, p1, only)
         for dz in (0, 1, 2, 3):
             add("z-", dz, 0, "h" if dz == 3 else "w", 1, 0, p1)
+        add("z-", 3, 0, "l", 1, 0, p1, ahead(name, 0))
         for dz in range(NZ):
             add("y+", dz, 0, "w", 0, -1, p2)
             add("y-", dz, 0, "w", 0, 1, p2)
@@ -113,11 +130,13 @@
         for n, first in (("A", "y"), ("B", "z")):
             tasks.append(Task("mm" + n, u, xkeys + unit_keys(n, first, u), [("mm", n, u)], 5))
             done.append(("mm", n, u))
-    tasks.append(Task("silu", 0, done, [("H",)], 5))
+    tasks.append(Task("silu", 1, done, [("H", 1)], 5))
+    tasks.append(Task("silu", 0, done, [("H", 0)], 5))
     for u in range(NZ):
-        dk = [("H",)] + unit_keys("DA", "y", u) + unit_keys("DB", "z", u)
-        tasks.append(Task("dn", u, dk, [("P", u)], 5))
-        sends.append(Send("s", ("S", u), ("S", u), 4 * 96 * 256 * 2, [("P", u)], 0))
+        dk = unit_keys("DA", "y", u) + unit_keys("DB", "z", u)
+        tasks.append(Task("dns", u, [("H", 1)] + dk, [("PS", u)], 4.5))
+        tasks.append(Task("dno", u, [("H", 0)] + dk, [("P", u)], 5))
+        sends.append(Send("s", ("S", u), ("S", u), 4 * 96 * 256 * 2, [("PS", u)], 0))
         tasks.append(Task("red1", u, [("P", u), ("S", u)], [("T", u)], 4))
         sends.append(Send("x-", ("T", u, 0), ("R", u, 0), 48 * 512, [("T", u)], 0))
         sends.append(Send("x+", ("T", u, 1), ("R", u, 1), 48 * 512, [("T", u)], 0))
@@ -130,11 +149,15 @@
 
 def greedy(ops):
     known, free, order, t, left = {}, {}, [], 0.0, list(range(len(ops)))
+    missing = {}
+    for o in ops:
+        for k in [o.dst] if isinstance(o, Send) else o.gives:
+            missing[k] = missing.get(k, 0) + 1
     while left:
         best, soonest = None, None
         for i in left:
             o = ops[i]
-            if any(k not in known for k in o.deps):
+            if any(missing[k] for k in o.deps):
                 continue
             at = max([known[k] for k in o.deps], default=0.0)
             if isinstance(o, Send):
@@ -157,27 +180,30 @@
             t += ISSUE
             rate, lat = (SIB, LAT_SIB) if o.link == "s" else (ICI, LAT)
             free[o.link] = max(free.get(o.link, 0.0), t) + o.nbytes / rate
-            known[o.dst] = free[o.link] + lat
+            known[o.dst] = max(known.get(o.dst, 0.0), free[o.link] + lat)
+            missing[o.dst] -= 1
         else:
             t += o.dur
             for k in o.gives:
                 known[k] = t
+                missing[k] -= 1
     return order
 
 
 PLAN = (
-    178, 0, 68, 97, 64, 32, 33, 96, 179, 129, 8, 4, 36, 9, 72, 128, 132, 40, 130, 73,
-    100, 69, 1, 35, 99, 98, 34, 65, 5, 94, 131, 11, 93, 60, 12, 57, 41, 2, 53, 50,
-    30, 10, 107, 27, 37, 90, 14, 135, 47, 134, 6, 75, 124, 133, 66, 78, 76, 43, 26, 24,
-    61, 54, 79, 3, 13, 136, 58, 29, 51, 25, 92, 7, 31, 117, 48, 70, 137, 42, 62, 88,
-    28, 183, 180, 23, 194, 38, 44, 18, 55, 95, 195, 59, 111, 20, 15, 52, 182, 16, 45, 63,
-    19, 22, 21, 17, 39, 49, 114, 184, 81, 192, 185, 56, 104, 74, 71, 87, 125, 46, 112, 118,
-    121, 181, 89, 67, 77, 193, 190, 80, 101, 186, 91, 191, 82, 189, 108, 115, 187, 188, 122, 105,
-    196, 201, 143, 109, 84, 197, 138, 126, 225, 173, 119, 102, 221, 202, 144, 145, 123, 168, 205, 198,
-    140, 148, 139, 113, 106, 83, 116, 226, 174, 110, 175, 85, 222, 169, 170, 206, 149, 150, 120, 127,
-    86, 103, 203, 146, 147, 199, 141, 142, 217, 163, 227, 176, 177, 223, 209, 153, 218, 165, 164, 172,
-    213, 158, 171, 207, 204, 210, 155, 200, 154, 214, 160, 152, 159, 151, 219, 166, 228, 167, 211, 224,
-    157, 156, 215, 161, 162, 208, 220, 212, 216,
+    184, 0, 4, 33, 34, 76, 9, 71, 185, 41, 67, 134, 37, 135, 136, 101, 10, 100, 45, 36,
+    13, 35, 5, 63, 112, 12, 49, 72, 31, 138, 30, 1, 103, 53, 79, 60, 68, 14, 6, 139,
+    15, 98, 56, 64, 42, 16, 2, 46, 102, 27, 80, 137, 7, 140, 8, 11, 82, 19, 73, 50,
+    61, 32, 17, 38, 57, 24, 29, 3, 25, 69, 141, 120, 104, 99, 54, 43, 47, 142, 65, 75,
+    62, 22, 21, 143, 123, 26, 28, 187, 201, 51, 189, 86, 188, 58, 18, 92, 39, 186, 44, 55,
+    94, 130, 20, 191, 81, 116, 127, 190, 66, 77, 197, 23, 198, 97, 83, 48, 59, 85, 95, 78,
+    40, 108, 74, 105, 84, 70, 131, 52, 200, 113, 87, 199, 192, 96, 121, 128, 93, 196, 124, 195,
+    193, 117, 194, 202, 109, 239, 179, 106, 209, 149, 132, 88, 203, 125, 114, 91, 240, 122, 241, 181,
+    180, 118, 204, 144, 129, 89, 210, 110, 214, 154, 205, 211, 151, 150, 234, 174, 133, 206, 146, 145,
+    126, 215, 216, 156, 155, 90, 235, 119, 242, 183, 182, 219, 111, 159, 236, 176, 175, 107, 212, 153,
+    152, 115, 220, 221, 161, 160, 207, 148, 147, 229, 169, 217, 158, 157, 224, 164, 230, 225, 231, 170,
+    171, 226, 166, 165, 243, 237, 177, 178, 222, 208, 213, 163, 162, 232, 172, 173, 218, 227, 168, 167,
+    223, 233, 238, 228,
 )
 SENDS, TASKS = build()
 OPS = SENDS + TASKS
@@ -185,19 +211,24 @@
 
 
 def number():
-    links = ("y+", "y-", "z+", "z-", "x+", "x-", "s")
+    base = {l: sum(SLOT_COUNT[m] for m in LINKS[:i]) for i, l in enumerate(LINKS)}
     count, sems = {}, {}
     for o in ORDER:
         if isinstance(o, Send):
-            n = count.get(o.link, 0)
-            count[o.link] = n + 1
-            o.slot = links.index(o.link) * SLOTS + n % SLOTS
-            group = o.dst[:2] if o.dst[0] in ("R", "F") else o.dst
-            o.sem = sems.setdefault(group, len(sems))
-    return len(links) * SLOTS, len(sems)
+            if o.only != ():
+                n = count.get(o.link, 0)
+                count[o.link] = n + 1
+                o.slot = base[o.link] + n % SLOT_COUNT[o.link]
+            users = tuple(i for i, q in enumerate(ORDER) if o.dst in q.deps)
+            o.sem = sems.setdefault(users, len(sems))
+    return sum(SLOT_COUNT.values()), len(sems)
 
 
 N_SEND, N_RECV = number()
+
+
+def silu(v):
+    return 0.5 * v * (1.0 + jnp.tanh(0.5 * v))
 
 
 def nt(a, b):
@@ -290,7 +321,7 @@
             return copy(s, place(s.src), weight(name, dz, s.src[2], part))
         return copy(s, place(s.src), place(s.dst))
 
-    by_dst = {s.dst: s for s in SENDS}
+    by_dst = {q.dst: q for q in SENDS if q.only != ()}
     waited = set()
 
     def arrive(key):
@@ -300,12 +331,12 @@
         if s.sem in waited:
             return
         waited.add(s.sem)
-        if key[0] == "S":
-            ref = srecv.at[key[1]]
-        elif key[0] in ("R", "F"):
-            ref = (rrecv if key[0] == "R" else frecv).at[key[1]]
+        total = sum({q.dst: q.nbytes for q in SENDS if q.sem == s.sem}.values())
+        tall = [k for k in range(1, 9) if total % (8192 * k) == 0 and total // (512 * k) <= ALL_ROWS]
+        if total % 8192:
+            ref = place(key)
         else:
-            ref = place(key)
+            ref = xbuf.at[pl.ds(0, tall[0]), pl.ds(0, total // (512 * tall[0])), :]
         copy(s, ref, ref).wait_recv()
 
     first = {"A": True, "B": True}
@@ -342,29 +373,32 @@
             part = jnp.dot(xbuf[u], w[u], preferred_element_type=F32)
             acc[...] = part if start else acc[...] + part
         elif o.kind == "silu":
-            for load in loads[5:]:
-                load.wait()
+            if u == 1:
+                for load in loads[5:]:
+                    load.wait()
             gs, us = gsc[...].reshape(1, 704), usc[...].reshape(1, 704)
             mixed_scale = jnp.concatenate([gs[:, WA:], us[:, WA:]], axis=1)
             low = lax.broadcasted_iota(jnp.int32, (32, 128), 1) < 64
 
-            @pl.loop(0, ALL_ROWS // 32)
+            @pl.loop(0, 384 // 32)
             def _(i):
-                rows = pl.ds(pl.multiple_of(i * 32, 32), 32)
+                rows = pl.ds(pl.multiple_of(u * 384 + i * 32, 32), 32)
                 g = acca[rows, :] * gs[:, :WA]
                 v = accb[rows, pl.ds(0, WA)] * us[:, :WA]
-                hid[rows, pl.ds(0, WA)] = (g / (1.0 + jnp.exp(-g)) * v).astype(BF16)
+                hid[rows, pl.ds(0, WA)] = (silu(g) * v).astype(BF16)
                 m = accb[rows, pl.ds(WA, 128)] * mixed_scale
-                h = m / (1.0 + jnp.exp(-m)) * pltpu.roll(m, 64, 1)
+                h = silu(m) * pltpu.roll(m, 64, 1)
                 hid[rows, pl.ds(WA, 128)] = jnp.where(low, h, 0.0).astype(BF16)
-        elif o.kind == "dn":
+        elif o.kind in ("dns", "dno"):
             tiles = [dbuf[u, :, pl.ds(i * 64, 64), :].reshape(256, 128) for i in range(5)]
             left = dbuf[u, :, pl.ds(320, 32), :]
             right = pltpu.roll(left.astype(F32).reshape(128, 128), 64, 1).astype(BF16)
             tiles.append(jnp.concatenate([left, right.reshape(4, 32, 128)], axis=1).reshape(256, 128))
             w = jnp.concatenate(tiles, axis=1)
-            ssend[u] = nt(hid[pl.ds(384, 384), :], w).astype(BF16)
-            pown[u] = nt(hid[pl.ds(0, 384), :], w)
+            if o.kind == "dns":
+                ssend[u] = nt(hid[pl.ds(384, 384), :], w).astype(BF16)
+            else:
+                pown[u] = nt(hid[pl.ds(0, 384), :], w)
         elif o.kind == "red1":
             q = pown[u] + srecv[u].astype(F32)
             pown[u] = q
@@ -381,19 +415,36 @@
             cols = pl.ds(pl.multiple_of(((zlo + u) % NZ) * 256, 256), 256)
             out[:, cols] = (total * dsc[:, cols]).astype(BF16)
 
+    def active(s):
+        return (zg >= s.only[0]) & (zg <= s.only[-1])
+
+    def begin(s):
+        if s.only is None:
+            outgoing(s).start()
+        else:
+            pl.when(active(s))(lambda: outgoing(s).start())
+
+    def finish(s):
+        if s.only is None:
+            outgoing(s).wait_send()
+        else:
+            pl.when(active(s))(lambda: outgoing(s).wait_send())
+
     sent = {}
     for o in ORDER:
+        if isinstance(o, Send) and o.only == ():
+            continue
         for key in o.deps:
             arrive(key)
         if isinstance(o, Send):
             if o.slot in sent:
-                sent[o.slot].wait_send()
-            sent[o.slot] = outgoing(o)
-            sent[o.slot].start()
+                finish(sent[o.slot])
+            sent[o.slot] = o
+            begin(o)
         else:
             run(o)
-    for c_out in sent.values():
-        c_out.wait_send()
+    for o in sent.values():
+        finish(o)
 
 
 def on_device(

time: 77.6 us -> 76.1 us (0.981)
  Pallas kernels: 76.7 us -> 75.3 us
    pallas_call x1, Pallas kernels: 76.7 us -> 75.3 us  [on_device(): pl.pallas_call(kernel, out_shape=pltpu.VMEM((ROWS, D), BF16), in_specs=[h...]
where the time goes in v3:
time: 76.1 us; the launch traced here: 76 us
  Pallas kernels  75.3 us (99%)
    pallas_call x1, Pallas kernels, on_device(): pl.pallas_call(kernel, out_shape=pltpu.VMEM((ROWS, D), BF16), in_specs=[h...  75.3 us

profile of v3, /device:TPU:1, one launch (start us, length us, event | category | flops | bytes accessed | tf_op | source)
XLA Modules:
  0.0 76.0 jit_solution(3421136335398016550)
XLA Ops:
  0.0 75.3 %shard_map.82 = bf16[96,2048]{1,0:T(8,128)(2,1)S(1)} custom-call(bf16[96,2048]{1,0:T(8,128)(2,1)} %tok_in.1, f32[1,2048]{1,0:T(1,128)} %bitcast.4, f32[64,704]{1,0:T(8,128)} %gw_in.1, f32[64,704]{1,0:T(8,128)} %uw_in.1, f32[704]{0:T(1024)} %gsc_in.1, f32[704]{0:T(1024)} %usc_in.1, f32[64,704]{1,0:T(8,128)} %bitcast.3, f32[1,2048]{1,0:T(1,128)} %bitcast.5), custom_call_target="tpu_custom_call" | custom-call | tf_op jit(solution)/shard_map/pallas_call | solution.py:455
  75.3 0.7 copy.10

commit v4 on v3

--- a/solution.py
+++ b/solution.py
@@ -25,15 +25,16 @@
 }
 
 
-TURN = {("A", 0): 3, ("A", 1): 0, ("B", 0): 4, ("DA", 0): 3, ("DA", 1): 4, ("DB", 0): 2}
+TURN = {("A", 0): 0, ("A", 1): 3, ("B", 0): 2, ("DA", 0): 4, ("DA", 1): 4, ("DB", 0): 0}
+
+SPREAD = {("A", 7): 0, ("A", 6): 0, ("A", 5): 0, ("DA", 7): 0, ("DA", 6): 0, ("DA", 5): 0}
 
 
 def ahead(name, dy):
     return tuple(range(1, TURN[name, dy] + 1))
 
 
-def behind(name, dy):
-    n = TURN[name, dy]
+def behind(n):
     return tuple(range(n - 1, 15)) if n else None
 
 
@@ -76,10 +77,19 @@
         add("y-", 0, 0, "w", 0, 1, p1)
         add("y+", 0, 3, "l", 0, -1, p1)
         add("y-", 0, 1, "h", 0, 1, p1)
+        for dz in (7, 6, 5):
+            spread = tuple(range(SPREAD[name, dz]))
+            add("y+", dz, 0, "w", 0, -1, p2, spread)
+            add("y-", dz, 0, "w", 0, 1, p2, spread)
+            add("y+", dz, 3, "w", 0, -1, p2, spread)
         for dy in range(4):
             for dz in (0, 7, 6, 5):
                 if dz != 5 or dy in (0, 1):
-                    add("z+", dz, dy, "w", -1, 0, p2, behind(name, dy) if dz == 5 else None)
+                    if dz == 5:
+                        only = behind(TURN[name, dy])
+                    else:
+                        only = behind(SPREAD[name, (dz - 1) % NZ]) if dy else None
+                    add("z+", dz, dy, "w", -1, 0, p2, only)
             for dz in (0, 1, 2, 3):
                 if dz != 3 or dy in (2, 3):
                     add("z-", dz, dy, "w", 1, 0, p2)
@@ -87,7 +97,7 @@
                     add("z-", dz, dy, "w", 1, 0, p2, ahead(name, dy))
     else:
         for dz in (0, 7, 6, 5):
-            only = behind(name, 0) if dz == 5 else None
+            only = behind(TURN[name, 0]) if dz == 5 else None
             add("z+", dz, 0, "l" if dz == 5 else "w", -1, 0, p1, only)
         for dz in (0, 1, 2, 3):
             add("z-", dz, 0, "h" if dz == 3 else "w", 1, 0, p1)
@@ -108,8 +118,8 @@
     tasks.append(Task("norm", 0, [], [("own", "X")], -1))
     sends += weight_sends("B", "z", 64 * WB * 2, 0, 2)
     sends += weight_sends("A", "y", 64 * WA * 2, 0, 2)
-    sends += weight_sends("DB", "z", 224 * 256, 2.5, 3)
-    sends += weight_sends("DA", "y", 128 * 256, 2.5, 3)
+    sends += weight_sends("DB", "z", 256 * 256, 2.5, 3)
+    sends += weight_sends("DA", "y", 96 * 256, 2.5, 3)
 
     xb = 48 * D * 2
     ox = [("own", "X")]
@@ -191,19 +201,20 @@
 
 
 PLAN = (
-    184, 0, 4, 33, 34, 76, 9, 71, 185, 41, 67, 134, 37, 135, 136, 101, 10, 100, 45, 36,
-    13, 35, 5, 63, 112, 12, 49, 72, 31, 138, 30, 1, 103, 53, 79, 60, 68, 14, 6, 139,
-    15, 98, 56, 64, 42, 16, 2, 46, 102, 27, 80, 137, 7, 140, 8, 11, 82, 19, 73, 50,
-    61, 32, 17, 38, 57, 24, 29, 3, 25, 69, 141, 120, 104, 99, 54, 43, 47, 142, 65, 75,
-    62, 22, 21, 143, 123, 26, 28, 187, 201, 51, 189, 86, 188, 58, 18, 92, 39, 186, 44, 55,
-    94, 130, 20, 191, 81, 116, 127, 190, 66, 77, 197, 23, 198, 97, 83, 48, 59, 85, 95, 78,
-    40, 108, 74, 105, 84, 70, 131, 52, 200, 113, 87, 199, 192, 96, 121, 128, 93, 196, 124, 195,
-    193, 117, 194, 202, 109, 239, 179, 106, 209, 149, 132, 88, 203, 125, 114, 91, 240, 122, 241, 181,
-    180, 118, 204, 144, 129, 89, 210, 110, 214, 154, 205, 211, 151, 150, 234, 174, 133, 206, 146, 145,
-    126, 215, 216, 156, 155, 90, 235, 119, 242, 183, 182, 219, 111, 159, 236, 176, 175, 107, 212, 153,
-    152, 115, 220, 221, 161, 160, 207, 148, 147, 229, 169, 217, 158, 157, 224, 164, 230, 225, 231, 170,
-    171, 226, 166, 165, 243, 237, 177, 178, 222, 208, 213, 163, 162, 232, 172, 173, 218, 227, 168, 167,
-    223, 233, 238, 228,
+    202, 0, 4, 33, 34, 76, 203, 9, 126, 10, 154, 80, 50, 46, 86, 155, 85, 36, 54, 5,
+    72, 58, 12, 110, 153, 1, 31, 109, 69, 35, 88, 89, 81, 152, 77, 15, 11, 6, 158, 16,
+    38, 13, 65, 37, 62, 73, 157, 2, 51, 27, 156, 59, 28, 32, 70, 55, 134, 160, 111, 47,
+    17, 7, 39, 18, 91, 19, 29, 40, 42, 161, 107, 66, 3, 78, 159, 74, 63, 8, 122, 14,
+    30, 41, 25, 112, 56, 20, 113, 60, 48, 43, 145, 148, 21, 130, 103, 67, 90, 205, 24, 82,
+    207, 218, 71, 204, 216, 61, 26, 64, 138, 22, 52, 23, 44, 106, 93, 209, 149, 114, 53, 141,
+    49, 57, 108, 75, 131, 87, 219, 105, 45, 92, 211, 68, 115, 206, 95, 217, 123, 127, 79, 215,
+    117, 208, 139, 83, 146, 214, 210, 101, 142, 104, 213, 135, 212, 116, 220, 227, 167, 124, 132, 150,
+    221, 257, 84, 97, 197, 143, 232, 172, 118, 140, 128, 228, 229, 168, 169, 120, 96, 147, 136, 94,
+    222, 162, 100, 258, 259, 199, 198, 233, 234, 174, 173, 102, 223, 224, 163, 164, 98, 151, 99, 230,
+    171, 170, 129, 252, 192, 119, 144, 253, 260, 201, 200, 125, 137, 237, 177, 235, 176, 133, 175, 254,
+    193, 121, 225, 194, 238, 247, 187, 239, 179, 178, 165, 166, 242, 182, 231, 248, 249, 188, 189, 243,
+    244, 184, 183, 255, 196, 195, 236, 240, 180, 181, 261, 226, 250, 191, 190, 245, 185, 186, 251, 256,
+    241, 246,
 )
 SENDS, TASKS = build()
 OPS = SENDS + TASKS
@@ -279,8 +290,8 @@
     yabs = [(y + dy) % NY for dy in range(NY)]
     parts = {
         "A": {"w": (0, 64), "l": (0, 32), "h": (32, 32)},
-        "DA": {"w": (0, 128), "l": (0, 64), "h": (64, 64)},
-        "DB": {"w": (128, 224), "l": (128, 112), "h": (240, 112)},
+        "DA": {"w": (0, 96), "l": (0, 48), "h": (48, 48)},
+        "DB": {"w": (96, 256), "l": (96, 128), "h": (224, 128)},
     }
     parts["B"] = parts["A"]
 

time: 76.1 us -> 75.5 us (level)
  no operation moved by 1% of the time
where the time goes in v4:
time: 75.5 us; the launch traced here: 75.3 us
  Pallas kernels  74.6 us (99%)
    pallas_call x1, Pallas kernels, on_device(): pl.pallas_call(kernel, out_shape=pltpu.VMEM((ROWS, D), BF16), in_specs=[h...  74.6 us

profile of v4, /device:TPU:1, one launch (start us, length us, event | category | flops | bytes accessed | tf_op | source)
XLA Modules:
  0.0 75.3 jit_solution(3377389272425090413)
XLA Ops:
  0.0 74.6 %shard_map.82 = bf16[96,2048]{1,0:T(8,128)(2,1)S(1)} custom-call(bf16[96,2048]{1,0:T(8,128)(2,1)} %tok_in.1, f32[1,2048]{1,0:T(1,128)} %bitcast.4, f32[64,704]{1,0:T(8,128)} %gw_in.1, f32[64,704]{1,0:T(8,128)} %uw_in.1, f32[704]{0:T(1024)} %gsc_in.1, f32[704]{0:T(1024)} %usc_in.1, f32[64,704]{1,0:T(8,128)} %bitcast.3, f32[1,2048]{1,0:T(1,128)} %bitcast.5), custom_call_target="tpu_custom_call" | custom-call | tf_op jit(solution)/shard_map/pallas_call | solution.py:466
  74.6 0.7 copy.10
